TPU v7x, 32 devices: a whole 2x2x4 slice. The times are simulated.
32 devices in a mesh: fs: 8 (over z, x), tp: 4 (over y, core).
Axes of the slice: x: 2, y: 2, z: 4, core: 2. Of those that a mesh axis runs over, the one named last changes fastest.
Arguments:
- tokens: bfloat16 [8192, 2048], P('fs', 'tp'), may hold values from -50 to 50
- norm_gain: float32 [2048], P('fs'), may hold values from 0.1 to 1.9
- gate_weight: float32 [2048, 2816], P('fs', 'tp'), may hold values from -0.125 to 0.125
- up_weight: float32 [2048, 2816], P('fs', 'tp'), may hold values from -0.125 to 0.125
- down_weight: float32 [2816, 2048], P('fs', 'tp'), may hold values from -0.109375 to 0.109375
Outputs:
- gate_sampler: bfloat16 [2048, 2816], P(None, 'tp')
- up_sampler: bfloat16 [2048, 2816], P(None, 'tp')
- down_sampler: bfloat16 [2816, 2048], P('tp')
- mixed: bfloat16 [8192, 2048], P('fs', 'tp')
All inputs are finite; a program needn't handle non-finite values.
Results may differ from a plain program's by a relative error of at most 0.0095.
Values may be sent and summed in bfloat16 or wider, within the bound.
A program may use at most 128 MiB of HBM per device.

v0:
```python
import jax
import jax.numpy as jnp
from jax import lax
from jax.sharding import PartitionSpec as P

norm_eps = 1e-06


def shards(tokens, norm_gain, gate_weight, up_weight, down_weight):
    gate_local = (norm_gain[:, None] * gate_weight).astype(jnp.bfloat16)
    up_local = (norm_gain[:, None] * up_weight).astype(jnp.bfloat16)
    down_local = down_weight.astype(jnp.bfloat16)
    gathered = lax.all_gather(tokens, "tp", axis=1, tiled=True)
    floated = gathered.astype(jnp.float32)
    normed = (
        floated * lax.rsqrt(jnp.mean(floated * floated, axis=-1, keepdims=True) + norm_eps)
    ).astype(jnp.bfloat16)
    gate_sampler, up_sampler = (
        lax.all_gather(gate_local, "fs", axis=0, tiled=True),
        lax.all_gather(up_local, "fs", axis=0, tiled=True),
    )
    gate = jnp.dot(normed, gate_sampler, preferred_element_type=jnp.float32)
    up = jnp.dot(normed, up_sampler, preferred_element_type=jnp.float32)
    hidden = (jax.nn.silu(gate) * up).astype(jnp.bfloat16)
    down_columns = lax.all_gather(down_local, "fs", axis=0, tiled=True)
    down_sampler = lax.all_to_all(down_columns, "tp", split_axis=0, concat_axis=1, tiled=True)
    partial_value = jnp.dot(
        lax.all_gather(hidden, "tp", axis=1, tiled=True),
        down_columns,
        preferred_element_type=jnp.float32,
    ).astype(jnp.bfloat16)
    partial_value = lax.optimization_barrier(partial_value)
    summed = partial_value.astype(jnp.float32)
    return (gate_sampler, up_sampler, down_sampler, summed.astype(jnp.bfloat16))


def solution(mesh):
    return jax.shard_map(
        shards,
        mesh=mesh,
        in_specs=(P("fs", "tp"), P("fs"), P("fs", "tp"), P("fs", "tp"), P("fs", "tp")),
        out_specs=(P(None, "tp"), P(None, "tp"), P("tp", None), P("fs", "tp")),
        check_vma=False,
    )
```

profile of v0, /device:TPU:0, one launch (start us, length us, event | category | flops | bytes accessed | tf_op | source)
XLA Modules:
  0.0 316.4 jit_solution(10165208772231586884)
XLA Ops:
  7.2 0.0 all-gather.12.cloned.1.call-start
  7.2 0.7 all-gather.12.cloned.1.call-update
  7.9 0.0 all-gather.6.cloned.1.call-start
  8.0 2.3 multiply_convert_fusion.1
  10.3 0.0 all-gather.8.cloned.1.call-start
  10.3 0.7 all-gather.8.cloned.1.call-update
  11.0 0.0 all-gather.10.cloned.1.call-start
  11.1 0.8 convert_element_type.25
  11.9 0.0 all-gather.14.cloned.1.call-start
  11.9 34.8 %all-gather.12.cloned.1.call-done = bf16[1024,2048]{1,0:T(8,128)(2,1)} async-done(((bf16[1024,512]{1,0:T(8,128)(2,1)}), bf16[1024,2048]{1,0:T(8,128)(2,1)}) %all-gather.12.cloned.1.call-update) | async-done | bytes 4194320 | tf_op jit(solution)/shard_map/all_gather | solution.py:13
  46.8 3.1 fusion
  49.8 59.1 %all-gather.6.cloned.1.call-done = bf16[2048,704]{0,1:T(8,128)(2,1)} async-done(((bf16[256,704]{0,1:T(8,128)(2,1)}), bf16[2048,704]{0,1:T(8,128)(2,1)}) %all-gather.6.cloned.1.call-update) | async-done | bytes 2883600 | tf_op jit(solution)/shard_map/all_gather | solution.py:19
  109.0 6.3 %fusion.3 = f32[1024,704]{0,1:T(8,128)S(1)} fusion(bf16[2048,704]{0,1:T(8,128)(2,1)} %all-gather.6.cloned.1.call-done, bf16[1024,2048]{1,0:T(8,128)(2,1)} %all-gather.12.cloned.1.call-done, f32[1024]{0:T(1024)S(1)} %add_rsqrt_fusion), kind=kOutput, calls=%fused_computation.5 | convolution fusion | flops 2959081472 | bytes 9965568 | tf_op jit(solution)/shard_map/dot_general | solution.py:22
  115.2 54.1 %all-gather.8.cloned.1.call-done = bf16[2048,704]{0,1:T(8,128)(2,1)} async-done(((bf16[256,704]{0,1:T(8,128)(2,1)}), bf16[2048,704]{0,1:T(8,128)(2,1)}) %all-gather.8.cloned.1.call-update) | async-done | bytes 2883600 | tf_op jit(solution)/shard_map/all_gather | solution.py:20
  169.4 7.7 %multiply_convert_fusion = bf16[1024,704]{0,1:T(8,128)(2,1)} fusion(f32[1024,704]{0,1:T(8,128)S(1)} %fusion.3, bf16[2048,704]{0,1:T(8,128)(2,1)} %all-gather.8.cloned.1.call-done, bf16[1024,2048]{1,0:T(8,128)(2,1)} %all-gather.12.cloned.1.call-done, f32[1024]{0:T(1024)S(1)} %add_rsqrt_fusion), kind=kOutput, calls=%fused_computation.4 | convolution fusion | flops 2963406848 | bytes 11407360 | tf_op jit(solution)/shard_map/dot_general | solution.py:23
  177.1 0.0 all-gather.14.cloned.1.call-update
  177.1 50.4 %all-gather.10.cloned.1.call-done = bf16[2816,512]{1,0:T(8,128)(2,1)} async-done(((bf16[352,512]{1,0:T(8,128)(2,1)}), bf16[2816,512]{1,0:T(8,128)(2,1)}) %all-gather.10.cloned.1.call-update) | async-done | bytes 2883600 | tf_op jit(solution)/shard_map/all_gather | solution.py:25
  227.5 64.5 %all_to_all.19 = bf16[4,704,512]{2,1,0:T(8,128)(2,1)S(1)} all-to-all(bf16[4,704,512]{2,1,0:T(8,128)(2,1)} %bitcast.9), channel_id=1, replica_groups=mesh['fs'=8,'tp'=4] {'tp'}, dimensions={0} | all-to-all | bytes 5767168 | tf_op jit(solution)/shard_map/all_to_all | solution.py:26
  292.0 2.0 copy.11
  294.1 3.8 %all-gather.14.cloned.1.call-done = bf16[1024,2816]{0,1:T(8,128)(2,1)} async-done(((bf16[1024,704]{0,1:T(8,128)(2,1)}), bf16[1024,2816]{0,1:T(8,128)(2,1)}) %all-gather.14.cloned.1.call-update) | async-done | bytes 5767184 | tf_op jit(solution)/shard_map/all_gather | solution.py:28
  297.8 7.7 %convolution_convert_fusion = bf16[1024,512]{1,0:T(8,128)(2,1)} fusion(bf16[1024,2816]{0,1:T(8,128)(2,1)} %all-gather.14.cloned.1.call-done, bf16[2816,512]{1,0:T(8,128)(2,1)} %all-gather.10.cloned.1.call-done), kind=kOutput, calls=%fused_computation.6 | convolution fusion | flops 2953314304 | bytes 9699328 | tf_op jit(solution)/shard_map/dot_general | solution.py:27
  305.5 1.6 copy.14
  307.0 1.3 copy-done.1
  308.3 1.6 copy.15
  (8 shorter events, 0.0 us)
Async XLA Ops:
  7.2 3.9 %copy-start.2 = (f32[352,512]{1,0:T(8,128)S(1)}, f32[352,512]{1,0:T(8,128)}, u32[]{:S(2)}) copy-start(f32[352,512]{1,0:T(8,128)} %param.9) | copy-start | bytes 2162692
  7.2 39.6 %all-gather.12.cloned.1.call-start = ((), (), s32[]{:S(2)}) async-start(), calls=%async_computation.4 | async-start | bytes 5242880 | tf_op jit(solution)/shard_map/all_gather | solution.py:13
  7.9 101.1 %all-gather.6.cloned.1.call-start = ((), (), s32[]{:S(2)}) async-start(), calls=%async_computation.1 | async-start | bytes 3244032 | tf_op jit(solution)/shard_map/all_gather | solution.py:19
  10.3 159.1 %all-gather.8.cloned.1.call-start = ((), (), s32[]{:S(2)}) async-start(), calls=%async_computation.2 | async-start | bytes 3244032 | tf_op jit(solution)/shard_map/all_gather | solution.py:20
  11.0 216.5 %all-gather.10.cloned.1.call-start = ((), (), s32[]{:S(2)}) async-start(), calls=%async_computation.3 | async-start | bytes 3244032 | tf_op jit(solution)/shard_map/all_gather | solution.py:25
  11.9 285.9 %all-gather.14.cloned.1.call-start = ((), (), s32[]{:S(2)}) async-start(), calls=%async_computation.5 | async-start | bytes 7208960 | tf_op jit(solution)/shard_map/all_gather | solution.py:28
  294.1 11.4 %copy-start = (bf16[2048,704]{0,1:T(8,128)(2,1)S(1)}, bf16[2048,704]{0,1:T(8,128)(2,1)}, u32[]{:S(2)}) copy-start(bf16[2048,704]{0,1:T(8,128)(2,1)} %all-gather.6.cloned.1.call-done) | copy-start | bytes 8650756
  305.5 2.9 copy-start.1
Sparse Core Ops, SparseCore 0:
  9.5 37.1 all-gather.11
  49.4 59.5 all-gather.5
  111.6 57.7 all-gather.7
  172.0 55.4 all-gather.9
  229.5 68.2 all-gather.13
where the time goes:
time: 317 us; the launch traced here: 316 us
  waiting for transfers between devices  204 us (64%)
  blocking collectives  64.5 us (20%)
  matrix products  21.7 us (7%)
  between operations  13.8 us (4%)
  local copies, waits for them, and re-layouts  6.45 us (2%)
  other arithmetic  6.17 us (2%)
    all_to_all x1, blocking collectives, shards(): lax.all_to_all(down_columns, 'tp', split_axis=0, concat_axis=1, tiled=True)  64.5 us
    all_gather x1, waiting for transfers between devices, shards(): lax.all_gather(gate_local, 'fs', axis=0, tiled=True)  59.1 us
    all_gather x1, waiting for transfers between devices, shards(): lax.all_gather(up_local, 'fs', axis=0, tiled=True)  54.1 us
    all_gather x1, waiting for transfers between devices, shards(): down_columns = lax.all_gather(down_local, 'fs', axis=0, tiled=True)  50.4 us
    all_gather x1, waiting for transfers between devices, shards(): gathered = lax.all_gather(tokens, 'tp', axis=1, tiled=True)  34.8 us
    dot_general x1, matrix products, shards(): up = jnp.dot(normed, up_sampler, preferred_element_type=jnp.float32)  7.73 us
    dot_general x1, matrix products, shards(): jnp.dot(lax.all_gather(hidden, 'tp', axis=1, tiled=True), down_columns, p...  7.65 us
  transfers between devices with their start and end apart: 5, of which 5 were waited for; matrix products, arithmetic and copies ran while one was open for 7% of the time, Pallas kernels for 0%

commit v1 on v0

--- a/solution.py
+++ b/solution.py
@@ -10,7 +10,7 @@
     gate_local = (norm_gain[:, None] * gate_weight).astype(jnp.bfloat16)
     up_local = (norm_gain[:, None] * up_weight).astype(jnp.bfloat16)
     down_local = down_weight.astype(jnp.bfloat16)
-    gathered = lax.all_gather(tokens, "tp", axis=1, tiled=True)
+    gathered = jnp.concatenate(lax.all_gather(tokens, "tp"), axis=1)
     floated = gathered.astype(jnp.float32)
     normed = (
         floated * lax.rsqrt(jnp.mean(floated * floated, axis=-1, keepdims=True) + norm_eps)

time: 317 us -> 317 us (level)
  waiting for transfers between devices: 204 us -> 182 us
  other arithmetic: 6.17 us -> 19.5 us
  local copies, waits for them, and re-layouts: 6.45 us -> 15.3 us
    all_gather x1, waiting for transfers between devices: 59.1 us -> 37 us  [shards(): lax.all_gather(gate_local, 'fs', axis=0, tiled=True)]
    convert_element_type x0 -> x2, other arithmetic: none -> 13.3 us  [the longest x1 6.66 us: shards(): normed = (floated * lax.rsqrt(jnp.mean(floated * floated, axis=-1, keepdi...]
    convert_element_type x0 -> x1, local copies, waits for them, and re-layouts: none -> 8.82 us  [shards(): floated = gathered.astype(jnp.float32)]
  transfers between devices with their start and end apart: 5 -> 5, of which waited for: 5 -> 5; matrix products, arithmetic and copies ran while one was open for 7% -> 14% of each run, Pallas kernels for 0% -> 0%
where the time goes in v1:
time: 317 us; the launch traced here: 316 us
  waiting for transfers between devices  182 us (57%)
  blocking collectives  64.5 us (20%)
  matrix products  20.9 us (7%)
  other arithmetic  19.5 us (6%)
  local copies, waits for them, and re-layouts  15.3 us (5%)
  between operations  13.8 us (4%)
    all_to_all x1, blocking collectives, shards(): lax.all_to_all(down_columns, 'tp', split_axis=0, concat_axis=1, tiled=True)  64.5 us
    all_gather x1, waiting for transfers between devices, shards(): lax.all_gather(up_local, 'fs', axis=0, tiled=True)  54.6 us
    all_gather x1, waiting for transfers between devices, shards(): down_columns = lax.all_gather(down_local, 'fs', axis=0, tiled=True)  50.6 us
    all_gather x1, waiting for transfers between devices, shards(): lax.all_gather(gate_local, 'fs', axis=0, tiled=True)  37 us
    all_gather x1, waiting for transfers between devices, shards(): gathered = jnp.concatenate(lax.all_gather(tokens, 'tp'), axis=1)  34.8 us
    convert_element_type x1, local copies, waits for them, and re-layouts, shards(): floated = gathered.astype(jnp.float32)  8.82 us
    dot_general x1, matrix products, shards(): jnp.dot(lax.all_gather(hidden, 'tp', axis=1, tiled=True), down_columns, p...  7.65 us
    dot_general x1, matrix products, shards(): up = jnp.dot(normed, up_sampler, preferred_element_type=jnp.float32)  7.49 us
  transfers between devices with their start and end apart: 5, of which 5 were waited for; matrix products, arithmetic and copies ran while one was open for 14% of the time, Pallas kernels for 0%

profile of v1, /device:TPU:0, one launch (start us, length us, event | category | flops | bytes accessed | tf_op | source)
XLA Modules:
  0.0 316.4 jit_solution(17140836978841612080)
XLA Ops:
  7.2 0.7 all-gather.15.cloned.1.call-update
  7.9 0.0 all-gather.7.cloned.1.call-start
  8.0 2.3 multiply_convert_fusion.1
  10.3 0.0 all-gather.9.cloned.1.call-start
  10.3 0.7 all-gather.9.cloned.1.call-update
  11.1 0.8 convert_element_type.35
  11.9 0.0 all-gather.13.cloned.1.call-start
  11.9 34.8 %all-gather.15.cloned.1.call-done = bf16[4096,512]{1,0:T(8,128)(2,1)} async-done(((bf16[1024,512]{1,0:T(8,128)(2,1)}), bf16[4096,512]{1,0:T(8,128)(2,1)}) %all-gather.15.cloned.1.call-update) | async-done | bytes 4194320 | tf_op jit(solution)/shard_map/all_gather | solution.py:13
  46.8 6.6 %convert_bitcast_fusion = f32[1024,4,512]{2,0,1:T(8,128)} fusion(bf16[4096,512]{1,0:T(8,128)(2,1)} %all-gather.15.cloned.1.call-done), kind=kLoop, calls=%fused_computation.1 | loop fusion | flops 2097152 | bytes 12582912 | tf_op jit(solution)/shard_map/convert_element_type | solution.py:14
  53.4 8.8 %copy.15 = f32[1024,4,512]{0,2,1:T(8,128)} copy(f32[1024,4,512]{2,0,1:T(8,128)} %convert_bitcast_fusion) | data formatting | bytes 16777216 | tf_op jit(solution)/shard_map/convert_element_type | solution.py:14
  62.2 3.1 fusion
  65.3 6.7 %fusion.1 = bf16[1024,2048]{0,1:T(8,128)(2,1)} fusion(f32[1024,4,512]{0,2,1:T(8,128)} %copy.15, f32[1024]{0:T(1024)S(1)} %add_rsqrt_fusion), kind=kLoop, calls=%fused_computation.4 | loop fusion | flops 4194304 | bytes 12587008 | tf_op jit(solution)/shard_map/convert_element_type | solution.py:17
  71.9 37.0 %all-gather.7.cloned.1.call-done = bf16[2048,704]{0,1:T(8,128)(2,1)} async-done(((bf16[256,704]{0,1:T(8,128)(2,1)}), bf16[2048,704]{0,1:T(8,128)(2,1)}) %all-gather.7.cloned.1.call-update) | async-done | bytes 2883600 | tf_op jit(solution)/shard_map/all_gather | solution.py:19
  109.0 5.8 %fusion.2 = f32[1024,704]{0,1:T(8,128)S(1)} fusion(bf16[2048,704]{0,1:T(8,128)(2,1)} %all-gather.7.cloned.1.call-done, bf16[1024,2048]{0,1:T(8,128)(2,1)} %fusion.1), kind=kOutput, calls=%fused_computation.10 | convolution fusion | flops 2952790016 | bytes 9961472 | tf_op jit(solution)/shard_map/dot_general | solution.py:22
  114.7 54.6 %all-gather.9.cloned.1.call-done = bf16[2048,704]{0,1:T(8,128)(2,1)} async-done(((bf16[256,704]{0,1:T(8,128)(2,1)}), bf16[2048,704]{0,1:T(8,128)(2,1)}) %all-gather.9.cloned.1.call-update) | async-done | bytes 2883600 | tf_op jit(solution)/shard_map/all_gather | solution.py:20
  169.4 7.5 %multiply_convert_fusion = bf16[1024,704]{0,1:T(8,128)(2,1)} fusion(f32[1024,704]{0,1:T(8,128)S(1)} %fusion.2, bf16[2048,704]{0,1:T(8,128)(2,1)} %all-gather.9.cloned.1.call-done, bf16[1024,2048]{0,1:T(8,128)(2,1)} %fusion.1), kind=kOutput, calls=%fused_computation.5 | convolution fusion | flops 2957115392 | bytes 11403264 | tf_op jit(solution)/shard_map/dot_general | solution.py:23
  176.9 50.6 %all-gather.11.cloned.1.call-done = bf16[2816,512]{1,0:T(8,128)(2,1)} async-done(((bf16[352,512]{1,0:T(8,128)(2,1)}), bf16[2816,512]{1,0:T(8,128)(2,1)}) %all-gather.11.cloned.1.call-update) | async-done | bytes 2883600 | tf_op jit(solution)/shard_map/all_gather | solution.py:25
  227.5 64.5 %all_to_all.19 = bf16[4,704,512]{2,1,0:T(8,128)(2,1)S(1)} all-to-all(bf16[4,704,512]{2,1,0:T(8,128)(2,1)} %bitcast.21), channel_id=1, replica_groups=mesh['fs'=8,'tp'=4] {'tp'}, dimensions={0} | all-to-all | bytes 5767168 | tf_op jit(solution)/shard_map/all_to_all | solution.py:26
  292.0 2.0 copy.16
  294.1 3.8 %all-gather.13.cloned.1.call-done = bf16[1024,2816]{0,1:T(8,128)(2,1)} async-done(((bf16[1024,704]{0,1:T(8,128)(2,1)}), bf16[1024,2816]{0,1:T(8,128)(2,1)}) %all-gather.13.cloned.1.call-update) | async-done | bytes 5767184 | tf_op jit(solution)/shard_map/all_gather | solution.py:28
  297.8 7.7 %convolution_convert_fusion = bf16[1024,512]{1,0:T(8,128)(2,1)} fusion(bf16[1024,2816]{0,1:T(8,128)(2,1)} %all-gather.13.cloned.1.call-done, bf16[2816,512]{1,0:T(8,128)(2,1)} %all-gather.11.cloned.1.call-done), kind=kOutput, calls=%fused_computation.6 | convolution fusion | flops 2953314304 | bytes 9699328 | tf_op jit(solution)/shard_map/dot_general | solution.py:27
  305.5 1.6 copy.19
  307.0 1.3 copy-done.1
  308.3 1.6 copy.20
  (11 shorter events, 0.1 us)
Async XLA Ops:
  7.2 3.9 %copy-start.2 = (f32[352,512]{1,0:T(8,128)S(1)}, f32[352,512]{1,0:T(8,128)}, u32[]{:S(2)}) copy-start(f32[352,512]{1,0:T(8,128)} %param.9) | copy-start | bytes 2162692
  7.2 39.6 %all-gather.15.cloned.1.call-start = ((), (), s32[]{:S(2)}) async-start(), calls=%async_computation.5 | async-start | bytes 5242880 | tf_op jit(solution)/shard_map/all_gather | solution.py:13
  7.9 101.1 %all-gather.7.cloned.1.call-start = ((), (), s32[]{:S(2)}) async-start(), calls=%async_computation.1 | async-start | bytes 3244032 | tf_op jit(solution)/shard_map/all_gather | solution.py:19
  10.3 159.1 %all-gather.9.cloned.1.call-start = ((), (), s32[]{:S(2)}) async-start(), calls=%async_computation.2 | async-start | bytes 3244032 | tf_op jit(solution)/shard_map/all_gather | solution.py:20
  11.0 216.5 %all-gather.11.cloned.1.call-start = ((), (), s32[]{:S(2)}) async-start(), calls=%async_computation.3 | async-start | bytes 3244032 | tf_op jit(solution)/shard_map/all_gather | solution.py:25
  11.9 285.9 %all-gather.13.cloned.1.call-start = ((), (), s32[]{:S(2)}) async-start(), calls=%async_computation.4 | async-start | bytes 7208960 | tf_op jit(solution)/shard_map/all_gather | solution.py:28
  294.0 11.4 %copy-start = (bf16[2048,704]{0,1:T(8,128)(2,1)S(1)}, bf16[2048,704]{0,1:T(8,128)(2,1)}, u32[]{:S(2)}) copy-start(bf16[2048,704]{0,1:T(8,128)(2,1)} %all-gather.7.cloned.1.call-done) | copy-start | bytes 8650756
  305.5 2.9 copy-start.1
Sparse Core Ops, SparseCore 0:
  9.5 37.1 all-gather.14
  49.4 59.5 all-gather.6
  111.6 57.7 all-gather.8
  172.0 55.4 all-gather.10
  229.5 68.2 all-gather.12
